TPU v7x, 32 devices: a whole 2x2x4 slice. The times are simulated.
32 devices in a mesh: ep: 8 (over z, x), tp: 4 (over y, core).
Axes of the slice: x: 2, y: 2, z: 4, core: 2. Of those that a mesh axis runs over, the one named last changes fastest.
Arguments:
- tokens: bfloat16 [2048, 2048], P('ep')
- norm_gain: float32 [2048], replicated, may hold values from 0.1 to 1.9
- chosen: int32 [8, 256], replicated, may hold values from 0 to 2047, as said below
- route_weight: float32 [8, 256], P('ep'), may hold values from 0.2 to 1
- gate_weight: bfloat16 [8, 2048, 4096], P('ep', None, 'tp'), may hold values from -0.125 to 0.125
- up_weight: bfloat16 [8, 2048, 4096], P('ep', None, 'tp'), may hold values from -0.125 to 0.125
- down_weight: bfloat16 [8, 4096, 2048], P('ep', 'tp'), may hold values from -0.09375 to 0.09375
Outputs:
- combined: bfloat16 [2048, 2048], P('ep', 'tp')
Inputs may be any that keep to these rules, and one draw needn't show every extreme that they name: Each row of chosen lists 256 distinct token numbers in ascending order. Of the 256 consecutive tokens of one index of ep, a row holds at most 48, and every draw has rows that hold exactly 48 of them.
All inputs are finite; a program needn't handle non-finite values.
Results may differ from a plain program's by a relative error of at most 0.02.
Values may be sent and summed in bfloat16 or wider, within the bound.
A program may use at most 64 MiB of HBM per device.

v0:
```python
import jax
import jax.numpy as jnp
from jax import lax
from jax.sharding import PartitionSpec as P


def shards(tokens, norm_gain, chosen, route_weight, gate_weight, up_weight, down_weight):
    tok_rows, row_width = tokens.shape
    experts, capacity = chosen.shape
    ep_count = lax.axis_size("ep")
    tp_count = lax.axis_size("tp")
    owner_index = lax.axis_index("ep")
    slot_most = 3 * tok_rows // 16
    col_width = row_width // tp_count
    values = tokens.astype(jnp.float32)
    scale = lax.rsqrt(jnp.mean(values * values, axis=-1, keepdims=True) + 1e-06)
    normed = (values * scale * norm_gain[None, :]).astype(jnp.bfloat16)
    slot_steps = jnp.arange(slot_most, dtype=jnp.int32)
    first_token = owner_index * tok_rows
    run_start = jnp.sum((chosen < first_token).astype(jnp.int32), axis=1)
    run_end = jnp.sum((chosen < first_token + tok_rows).astype(jnp.int32), axis=1)
    run_count = run_end - run_start
    slot_live = slot_steps[None, :] < run_count[:, None]
    slot_place = jnp.minimum(run_start[:, None] + slot_steps[None, :], capacity - 1)
    slot_token = jnp.take_along_axis(chosen, slot_place, axis=1) - first_token
    slot_local = jnp.where(slot_live, slot_token, 0)
    my_chosen = lax.dynamic_index_in_dim(chosen, owner_index, 0, keepdims=False)
    block_edges = jnp.arange(ep_count, dtype=jnp.int32) * tok_rows
    src_start = jnp.sum((my_chosen[None, :] < block_edges[:, None]).astype(jnp.int32), axis=1)
    src_end = jnp.concatenate([src_start[1:], jnp.full((1,), capacity, jnp.int32)])
    gate_mat = gate_weight[0]
    up_mat = up_weight[0]
    down_mat = down_weight[0]
    outgoing = jnp.where(slot_live[:, :, None], normed[slot_local], jnp.zeros((), jnp.bfloat16))
    received = lax.all_to_all(outgoing, "ep", split_axis=0, concat_axis=0, tiled=True)
    source_block = my_chosen // tok_rows
    flat_index = (
        source_block * slot_most + jnp.arange(capacity, dtype=jnp.int32) - src_start[source_block]
    )
    expert_rows = received.reshape(-1, row_width)[flat_index]
    gate_pre = jnp.dot(expert_rows, gate_mat, preferred_element_type=jnp.float32)
    up_pre = jnp.dot(expert_rows, up_mat, preferred_element_type=jnp.float32)
    hidden = (jax.nn.silu(gate_pre) * up_pre).astype(jnp.bfloat16)
    summed_out = lax.psum_scatter(
        lax.dot_general(
            down_mat, hidden, (((0,), (1,)), ((), ())), preferred_element_type=jnp.float32
        ).astype(jnp.bfloat16),
        "tp",
        scatter_dimension=0,
        tiled=True,
    ).astype(jnp.float32)
    weighted = (summed_out.T * route_weight[0][:, None]).astype(jnp.bfloat16)
    back_place = jnp.minimum(src_start[:, None] + slot_steps[None, :], capacity - 1)
    back_live = slot_steps[None, :] < (src_end - src_start)[:, None]
    outgoing_back = jnp.where(
        back_live[:, :, None], weighted[back_place], jnp.zeros((), jnp.bfloat16)
    )
    returned = lax.all_to_all(outgoing_back, "ep", split_axis=0, concat_axis=0, tiled=True)
    target_row = jnp.where(slot_live, slot_token, tok_rows).reshape(-1)
    placement = (jnp.arange(tok_rows, dtype=jnp.int32)[:, None] == target_row[None, :]).astype(
        jnp.bfloat16
    )
    combined = jnp.dot(
        placement, returned.reshape(-1, col_width), preferred_element_type=jnp.float32
    )
    return combined.astype(jnp.bfloat16)


def solution(mesh):
    return jax.shard_map(
        shards,
        mesh=mesh,
        in_specs=(
            P("ep", None),
            P(),
            P(),
            P("ep", None),
            P("ep", None, "tp"),
            P("ep", None, "tp"),
            P("ep", "tp", None),
        ),
        out_specs=P("ep", "tp"),
        check_vma=False,
    )
```

profile of v0, /device:TPU:0, one launch (start us, length us, event | category | flops | bytes accessed | tf_op | source)
XLA Modules:
  0.0 124.3 jit_solution(5571698542294069855)
XLA Ops:
  6.5 0.0 copy-start
  6.5 0.9 convert_reduce_fusion.2
  7.4 0.1 shift-left_or_fusion
  7.5 0.1 reshape.457
  7.6 0.0 copy-done
  7.6 0.0 copy-start.1
  7.6 0.0 copy-start.2
  7.6 2.7 %gather_fusion.3 = s32[384]{0:T(512)S(1)} fusion(s32[8,256]{1,0:T(8,128)S(1)} %copy-done, s32[384]{0:T(512)S(1)} %reshape.457), kind=kCustom, calls=%fused_computation.3 | custom fusion | bytes 6144 | tf_op jit(solution)/shard_map/jit(take_along_axis)/gather | solution.py:25
  10.4 0.1 gather.24
  10.5 0.1 iota_compare_fusion.4
  10.6 0.1 compare_select_fusion.1
  10.6 0.1 reshape.420
  10.7 0.0 copy-done.1
  10.7 0.3 fusion.12
  11.0 0.0 copy-done.2
  11.0 0.3 fusion.14
  11.4 2.5 %gather_fusion = bf16[384,2048]{1,0:T(8,128)(2,1)S(1)} fusion(bf16[256,2048]{1,0:T(8,128)(2,1)S(1)} %fusion.14, s32[1024]{0:T(1024)S(1)} %pad_clamp_fusion.2), kind=kCustom, calls=%fused_computation | custom fusion | bytes 3147264 | tf_op jit(solution)/shard_map/gather | solution.py:34
  13.8 1.3 %broadcast_select_fusion = bf16[8,48,2048]{2,1,0:T(8,128)(2,1)} fusion(bf16[8,48,2048]{2,1,0:T(8,128)(2,1)S(1)} %bitcast.63, pred[8,48]{1,0:T(8,128)(4,1)S(1)} %iota_compare_fusion.4), kind=kLoop, calls=%fused_computation.17 | loop fusion | flops 786432 | bytes 3146112 | tf_op jit(solution)/shard_map/jit(_where)/select_n | solution.py:34
  15.2 7.3 %all-to-all-start = ((bf16[8,48,2048]{2,1,0:T(8,128)(2,1)}), bf16[8,48,2048]{2,1,0:T(8,128)(2,1)S(1)}, u32[]{:S(2)}, u32[]{:S(2)}) async-start(bf16[8,48,2048]{2,1,0:T(8,128)(2,1)} %broadcast_select_fusion), calls=%async_computation | async-start | bytes 3145728 | tf_op jit(solution)/shard_map/all_to_all | solution.py:35
  22.4 0.0 reduce-scatter.2.cloned.1.call-start
  22.5 0.2 convert_reduce_fusion
  22.7 0.7 fusion.30
  23.4 4.4 %compare_select_fusion.6 = (s32[256,1]{0,1:T(1,128)S(1)}, s32[256,1]{0,1:T(1,128)S(1)}) fusion(s32[]{:T(128)} %bitcast.5, s32[]{:T(128)} %bitcast.6, s32[]{:T(128)} %bitcast.7, s32[]{:T(128)} %bitcast.8, s32[]{:T(128)} %bitcast.9, s32[]{:T(128)} %bitcast.11, s32[]{:T(128)} %bitcast.10, s32[8,256]{1,0:T(8,128)S(1)} %copy-done, s32[]{:T(128)S(6)} %select_n.130), kind=kLoop, calls=%fused_computation.47 | loop fusion | flops 7680 | bytes 3104 | tf_op jit(solution)/shard_map/gather | solution.py:38
  27.8 0.7 broadcast_select_fusion.2
  28.5 31.0 %all-to-all-done = bf16[8,48,2048]{2,1,0:T(8,128)(2,1)S(1)} async-done(((bf16[8,48,2048]{2,1,0:T(8,128)(2,1)}), bf16[8,48,2048]{2,1,0:T(8,128)(2,1)S(1)}, u32[]{:S(2)}, u32[]{:S(2)}) %all-to-all-start) | async-done | bytes 1572896 | tf_op jit(solution)/shard_map/all_to_all | solution.py:35
  59.4 1.4 %gather_fusion.1 = bf16[256,2048]{1,0:T(8,128)(2,1)S(1)} fusion(bf16[384,2048]{1,0:T(8,128)(2,1)S(1)} %bitcast.62, s32[1024]{0:T(1024)S(1)} %pad_clamp_fusion.1), kind=kCustom, calls=%fused_computation.1 | custom fusion | bytes 2098176 | tf_op jit(solution)/shard_map/gather | solution.py:40
  60.8 3.5 %fusion.4 = f32[256,1024]{1,0:T(8,128)S(1)} fusion(bf16[256,2048]{1,0:T(8,128)(2,1)S(1)} %gather_fusion.1, bf16[1,2048,1024]{2,1,0:T(8,128)(2,1)} %param.11), kind=kOutput, calls=%fused_computation.8 | convolution fusion | flops 1073741824 | bytes 6291456 | tf_op jit(solution)/shard_map/dot_general | solution.py:41
  64.3 0.0 copy-start.3
  64.3 7.0 %fusion.9 = bf16[2048,256]{0,1:T(8,128)(2,1)} fusion(bf16[1,1024,2048]{2,1,0:T(8,128)(2,1)} %param.13, bf16[256,2048]{1,0:T(8,128)(2,1)S(1)} %gather_fusion.1, bf16[1,2048,1024]{2,1,0:T(8,128)(2,1)} %param.12, f32[256,1024]{1,0:T(8,128)S(1)} %fusion.4), kind=kOutput, calls=%fused_computation.13 | convolution fusion | flops 2149580800 | bytes 11534336 | tf_op jit(solution)/shard_map/dot_general | solution.py:45
  71.3 0.0 reduce-scatter.2.cloned.1.call-update
  71.3 0.1 slice.3
  71.4 0.1 compare_select_fusion
  71.5 0.1 reshape.451
  71.6 0.1 add_subtract_fusion
  71.6 0.1 iota_compare_fusion.3
  71.7 23.7 %reduce-scatter.2.cloned.1.call-done = bf16[512,256]{0,1:T(8,128)(2,1)} async-done(((bf16[2048,256]{0,1:T(8,128)(2,1)}), bf16[512,256]{0,1:T(8,128)(2,1)}) %reduce-scatter.2.cloned.1.call-update) | async-done | bytes 262160 | tf_op jit(solution)/shard_map/reduce_scatter | solution.py:44
  95.4 0.0 copy-done.3
  95.4 1.1 fusion.24
  96.5 2.1 %gather_fusion.2 = bf16[384,512]{1,0:T(8,128)(2,1)S(1)} fusion(bf16[256,512]{1,0:T(8,128)(2,1)S(1)} %fusion.24, s32[1024]{0:T(1024)S(1)} %pad_clamp_fusion), kind=kCustom, calls=%fused_computation.2 | custom fusion | bytes 787968 | tf_op jit(solution)/shard_map/gather | solution.py:56
  98.5 0.9 broadcast_select_fusion.1
  99.4 5.5 %all-to-all-start.1 = ((bf16[8,48,512]{2,1,0:T(8,128)(2,1)}), bf16[8,48,512]{2,1,0:T(8,128)(2,1)S(1)}, u32[]{:S(2)}, u32[]{:S(2)}) async-start(bf16[8,48,512]{2,1,0:T(8,128)(2,1)} %broadcast_select_fusion.1), calls=%async_computation.2 | async-start | bytes 786432 | tf_op jit(solution)/shard_map/all_to_all | solution.py:58
  104.9 0.1 lt.168
  105.0 0.1 add.172
  105.1 0.1 add.173
  105.2 0.1 lt.170
  105.3 11.2 %all-to-all-done.1 = bf16[8,48,512]{2,1,0:T(8,128)(2,1)S(1)} async-done(((bf16[8,48,512]{2,1,0:T(8,128)(2,1)}), bf16[8,48,512]{2,1,0:T(8,128)(2,1)S(1)}, u32[]{:S(2)}, u32[]{:S(2)}) %all-to-all-start.1) | async-done | bytes 393248 | tf_op jit(solution)/shard_map/all_to_all | solution.py:58
  116.4 1.0 convolution_convert_fusion
  (11 shorter events, 0.1 us)
Async XLA Ops:
  6.5 1.1 copy-start
  7.6 3.1 %copy-start.1 = (bf16[256,2048]{1,0:T(8,128)(2,1)S(1)}, bf16[256,2048]{1,0:T(8,128)(2,1)}, u32[]{:S(2)}) copy-start(bf16[256,2048]{1,0:T(8,128)(2,1)} %param.7) | copy-start | bytes 3145732
  7.6 3.4 %copy-start.2 = (f32[2048]{0:T(1024)S(1)}, f32[2048]{0:T(1024)}, u32[]{:S(2)}) copy-start(f32[2048]{0:T(1024)} %param.8) | copy-start | bytes 24580
  15.2 44.3 %all-to-all-start = ((bf16[8,48,2048]{2,1,0:T(8,128)(2,1)}), bf16[8,48,2048]{2,1,0:T(8,128)(2,1)S(1)}, u32[]{:S(2)}, u32[]{:S(2)}) async-start(bf16[8,48,2048]{2,1,0:T(8,128)(2,1)} %broadcast_select_fusion), calls=%async_computation | async-start | bytes 3145728 | tf_op jit(solution)/shard_map/all_to_all | solution.py:35
  22.4 73.0 %reduce-scatter.2.cloned.1.call-start = ((), (), s32[]{:S(2)}) async-start(), calls=%async_computation.3 | async-start | bytes 1310720 | tf_op jit(solution)/shard_map/reduce_scatter | solution.py:44
  64.3 31.1 %copy-start.3 = (f32[1,256]{1,0:T(1,128)S(1)}, f32[1,256]{1,0:T(1,128)}, u32[]{:S(2)}) copy-start(f32[1,256]{1,0:T(1,128)} %param.10) | copy-start | bytes 3076
  99.4 17.0 %all-to-all-start.1 = ((bf16[8,48,512]{2,1,0:T(8,128)(2,1)}), bf16[8,48,512]{2,1,0:T(8,128)(2,1)S(1)}, u32[]{:S(2)}, u32[]{:S(2)}) async-start(bf16[8,48,512]{2,1,0:T(8,128)(2,1)} %broadcast_select_fusion.1), calls=%async_computation.2 | async-start | bytes 786432 | tf_op jit(solution)/shard_map/all_to_all | solution.py:58
Sparse Core Ops, SparseCore 0:
  71.4 23.9 reduce-scatter.1
where the time goes:
time: 125 us; the launch traced here: 124 us
  waiting for transfers between devices  65.9 us (53%)
  between operations  13.6 us (11%)
  starting transfers between devices  12.8 us (10%)
  matrix products  11.5 us (9%)
  other arithmetic  10.5 us (8%)
  local copies, waits for them, and re-layouts  10 us (8%)
    all_to_all x1, waiting for transfers between devices, shards(): lax.all_to_all(outgoing, 'ep', split_axis=0, concat_axis=0, tiled=True)  31 us
    reduce_scatter x1, waiting for transfers between devices, shards(): lax.psum_scatter(lax.dot_general(down_mat, hidden, (((0,), (1,)), ((), ()...  23.7 us
    all_to_all x1, waiting for transfers between devices, shards(): lax.all_to_all(outgoing_back, 'ep', split_axis=0, concat_axis=0, tiled=True)  11.2 us
    all_to_all x1, starting transfers between devices, shards(): lax.all_to_all(outgoing, 'ep', split_axis=0, concat_axis=0, tiled=True)  7.28 us
    dot_general x1, matrix products, shards(): lax.dot_general(down_mat, hidden, (((0,), (1,)), ((), ())), preferred_ele...  7.02 us
    all_to_all x1, starting transfers between devices, shards(): lax.all_to_all(outgoing_back, 'ep', split_axis=0, concat_axis=0, tiled=True)  5.51 us
    gather x3, other arithmetic, shards(): src_start[source_block]  5.05 us
    dot_general x1, matrix products, shards(): jnp.dot(expert_rows, gate_mat, preferred_element_type=jnp.float32)  3.45 us
  transfers between devices with their start and end apart: 3, of which 3 were waited for; matrix products, arithmetic and copies ran while one was open for 5% of the time, Pallas kernels for 0%

commit v1 on v0

--- a/solution.py
+++ b/solution.py
@@ -1,8 +1,15 @@
+import functools
 import jax
 import jax.numpy as jnp
 from jax import lax
+from jax.experimental import pallas as pl
+from jax.experimental.pallas import tpu as pltpu
 from jax.sharding import PartitionSpec as P
 
+F32 = jnp.float32
+BF16 = jnp.bfloat16
+MESH = pl.DeviceIdType.MESH
+PARTS = 2
 
 def shards(tokens, norm_gain, chosen, route_weight, gate_weight, up_weight, down_weight):
     tok_rows, row_width = tokens.shape
@@ -66,9 +73,266 @@
     return combined.astype(jnp.bfloat16)
 
 
+def fused_kernel(
+    ep, nk, slots,
+    tokens, gain, chosen, route, gate_hbm, up_hbm, down_hbm, out,
+    gate_w, up_w, down_w, normed, pick, unpick, spread, gather, outgoing, received, rows, gate_acc,
+    up_acc, hidden, pair_out, pair_in, own_part, cross_out, cross_in, back_out, back_in,
+    w_sem, ep_send, ep_recv, y_send, y_recv, pair_send, pair_recv, relay_send, relay_recv,
+    ps_send, ps_recv, ys_send, ys_recv, back_send, back_recv,
+):
+    me = lax.axis_index("ep")
+    tp = lax.axis_index("tp")
+    y_pos = tp // 2
+    core = tp % 2
+    mate = y_pos * 2 + (1 - core)
+    across = (1 - y_pos) * 2 + core
+    diag = (1 - y_pos) * 2 + (1 - core)
+    tok_rows, width = tokens.shape
+    cap = chosen.shape[1]
+    quarter = width // 4
+    piece = quarter // nk
+    ff = gate_w.shape[1]
+    order = [d for d in sorted(range(1, ep), key=lambda d: abs(d - ep / 2))]
+
+    half = width // 2
+    loads = []
+    for i in range(2):
+        part = pl.ds(i * half, half)
+        loads.append(pltpu.make_async_copy(gate_hbm.at[0, part], gate_w.at[part], w_sem.at[3 * i]))
+        loads.append(pltpu.make_async_copy(up_hbm.at[0, part], up_w.at[part], w_sem.at[3 * i + 1]))
+    loads.append(pltpu.make_async_copy(down_hbm.at[0], down_w, w_sem.at[2]))
+    for load in loads:
+        load.start()
+
+    barrier = pltpu.get_barrier_semaphore()
+    for d in order:
+        pl.semaphore_signal(
+            barrier, inc=1, device_id={"ep": (me + d) % ep, "tp": tp}, device_id_type=MESH
+        )
+    for other in (mate, across):
+        pl.semaphore_signal(barrier, inc=1, device_id={"ep": me, "tp": other}, device_id_type=MESH)
+
+    my_cols = pl.ds(pl.multiple_of(tp * quarter, quarter), quarter)
+    my_gain = gain[:, my_cols]
+    step_rows = 32
+
+    @pl.loop(0, tok_rows // step_rows)
+    def _(r):
+        rs = pl.ds(pl.multiple_of(r * step_rows, step_rows), step_rows)
+        v = tokens[rs, :].astype(F32)
+        scale = lax.rsqrt(jnp.sum(v * v, axis=1, keepdims=True) * (1.0 / width) + 1e-06)
+        own = tokens[rs, my_cols].astype(F32)
+        normed[rs, :] = (own * scale * my_gain).astype(BF16)
+
+    first = me * tok_rows
+    lane = lax.broadcasted_iota(jnp.int32, (slots, cap), 1).astype(F32)
+    sub = lax.broadcasted_iota(jnp.int32, (slots, cap), 0).astype(F32)
+    tok_lane = lax.broadcasted_iota(jnp.int32, (slots, tok_rows), 1).astype(F32)
+    for e in range(ep):
+        row = chosen[e : e + 1, :]
+        local = (row - first).astype(F32)
+        start = jnp.sum(jnp.where(local < 0.0, 1.0, 0.0), axis=1, keepdims=True)
+        value = jnp.where((local >= 0.0) & (local < float(tok_rows)), local + 1.0, 0.0)
+        hit = lane == sub + start
+        slot_tok = jnp.sum(jnp.where(hit, value, 0.0), axis=1, keepdims=True) - 1.0
+        pick[e * slots : (e + 1) * slots, :] = jnp.where(tok_lane == slot_tok, 1.0, 0.0)
+
+    pick_b = pick[...].astype(BF16)
+    for k in range(nk):
+        got = jnp.dot(pick_b, normed[:, k * piece : (k + 1) * piece], preferred_element_type=F32)
+        outgoing[k] = got.astype(BF16).reshape(ep, slots, piece)
+
+    pl.semaphore_wait(barrier, ep + 1)
+
+    def ep_copy(buf_out, buf_in, s_sem, r_sem, k, d):
+        dest = (me + d) % ep
+        return pltpu.make_async_remote_copy(
+            src_ref=buf_out.at[k, dest], dst_ref=buf_in.at[k, me],
+            send_sem=s_sem.at[k, d], recv_sem=r_sem.at[k, d],
+            device_id={"ep": dest, "tp": tp}, device_id_type=MESH,
+        )
+
+    def tp_copy(a, b, s_sem, r_sem, k, other):
+        return pltpu.make_async_remote_copy(
+            src_ref=a, dst_ref=b, send_sem=s_sem.at[k], recv_sem=r_sem.at[k],
+            device_id={"ep": me, "tp": other}, device_id_type=MESH,
+        )
+
+    sends = []
+    dispatch = [[ep_copy(outgoing, received, ep_send, ep_recv, k, d) for d in order] for k in range(nk)]
+    for k in range(nk):
+        for c in dispatch[k]:
+            c.start()
+            sends.append(c)
+    for k in range(nk):
+        received[k, me] = outgoing[k, me]
+
+    mine = chosen[pl.ds(me, 1), :].astype(F32)
+    place = lax.broadcasted_iota(jnp.int32, (1, cap), 1).astype(F32)
+    slot_id = jnp.zeros((1, cap), F32)
+    for b in range(ep):
+        lo = float(b * tok_rows)
+        begin = jnp.sum(jnp.where(mine < lo, 1.0, 0.0), axis=1, keepdims=True)
+        inside = (mine >= lo) & (mine < lo + float(tok_rows))
+        slot_id = jnp.where(inside, place - begin + float(b * slots), slot_id)
+    slot_sub = lax.broadcasted_iota(jnp.int32, (ep * slots, cap), 0).astype(F32)
+    spread_f = jnp.where(slot_sub == slot_id, 1.0, 0.0)
+    spread[...] = spread_f.astype(BF16)
+    gather[...] = spread_f.T.astype(BF16)
+    unpick[...] = pick[...].T.astype(BF16)
+    eye_r = lax.broadcasted_iota(jnp.int32, (cap, cap), 0)
+    eye_c = lax.broadcasted_iota(jnp.int32, (cap, cap), 1)
+    weight = jnp.sum(jnp.where(eye_r == eye_c, route[...], 0.0), axis=1, keepdims=True)
+
+    def compact(k):
+        for c in dispatch[k]:
+            c.wait_recv()
+        got = jnp.dot(
+            gather[...], received[k].reshape(ep * slots, piece), preferred_element_type=F32
+        )
+        rows[tp, k] = got.astype(BF16)
+        for c in (
+            tp_copy(rows.at[tp, k], rows.at[tp, k], y_send, y_recv, k, across),
+            tp_copy(rows.at[tp, k], rows.at[tp, k], pair_send, pair_recv, k, mate),
+        ):
+            c.start()
+            sends.append(c)
+
+    def relay(k):
+        tp_copy(rows.at[tp, k], rows.at[across, k], y_send, y_recv, k, across).wait_recv()
+        c = tp_copy(rows.at[across, k], rows.at[across, k], relay_send, relay_recv, k, mate)
+        c.start()
+        sends.append(c)
+
+    tile = 256
+
+    def project(k):
+        if k == 0:
+            for load in loads[:4]:
+                load.wait()
+        tp_copy(rows.at[tp, k], rows.at[mate, k], pair_send, pair_recv, k, mate).wait_recv()
+        tp_copy(rows.at[tp, k], rows.at[diag, k], relay_send, relay_recv, k, mate).wait_recv()
+
+        @pl.loop(0, ff // tile)
+        def _(n):
+            cols = pl.ds(pl.multiple_of(n * tile, tile), tile)
+            g = jnp.zeros((cap, tile), F32) if k == 0 else gate_acc[:, cols]
+            u = jnp.zeros((cap, tile), F32) if k == 0 else up_acc[:, cols]
+            for t in range(4):
+                ks = slice(t * quarter + k * piece, t * quarter + (k + 1) * piece)
+                x = rows[t, k]
+                g = g + jnp.dot(x, gate_w[ks, cols], preferred_element_type=F32)
+                u = u + jnp.dot(x, up_w[ks, cols], preferred_element_type=F32)
+            if k < nk - 1:
+                gate_acc[:, cols] = g
+                up_acc[:, cols] = u
+            else:
+                hidden[:, cols] = (g / (1.0 + jnp.exp(-g)) * u).astype(BF16)
+
+    for k in range(nk + 2):
+        if k < nk:
+            compact(k)
+        if 1 <= k <= nk:
+            relay(k - 1)
+        if k >= 2:
+            project(k - 2)
+    loads[4].wait()
+
+    def down(t, k):
+        cols = pl.ds(pl.multiple_of(t * quarter + k * piece, piece), piece)
+        return jnp.dot(hidden[...], down_w[:, cols], preferred_element_type=F32)
+
+    other_y = 1 - y_pos
+    pair_c = [tp_copy(pair_out.at[k], pair_in.at[k], ps_send, ps_recv, k, mate) for k in range(nk)]
+    cross_c = [tp_copy(cross_out.at[k], cross_in.at[k], ys_send, ys_recv, k, across) for k in range(nk)]
+    for k in range(nk):
+        pair_out[k, 0] = down(diag, k).astype(BF16)
+        pair_out[k, 1] = down(mate, k).astype(BF16)
+        pair_c[k].start()
+        away = down(across, k)
+        own_part[k] = down(tp, k)
+        pair_c[k].wait_recv()
+        cross_out[k] = (away + pair_in[k, 0].astype(F32)).astype(BF16)
+        cross_c[k].start()
+    back = [[ep_copy(back_out, back_in, back_send, back_recv, k, d) for d in order] for k in range(nk)]
+    for k in range(nk):
+        near = own_part[k] + pair_in[k, 1].astype(F32)
+        cross_c[k].wait_recv()
+        total = (near + cross_in[k].astype(F32)) * weight
+        wide = jnp.dot(spread[...], total.astype(BF16), preferred_element_type=F32)
+        back_out[k] = wide.astype(BF16).reshape(ep, slots, piece)
+        for c in back[k]:
+            c.start()
+            sends.append(c)
+        back_in[k, me] = back_out[k, me]
+    for k in range(nk):
+        for c in back[k]:
+            c.wait_recv()
+        done = jnp.dot(
+            unpick[...], back_in[k].reshape(ep * slots, piece), preferred_element_type=F32
+        )
+        out[:, k * piece : (k + 1) * piece] = done.astype(BF16)
+    for c in sends + pair_c + cross_c:
+        c.wait_send()
+
+
+def fused(tokens, norm_gain, chosen, route_weight, gate_weight, up_weight, down_weight):
+    ep = lax.axis_size("ep")
+    nk = PARTS
+    tok_rows, width = tokens.shape
+    cap = chosen.shape[1]
+    slots = 3 * tok_rows // 16
+    quarter = width // lax.axis_size("tp")
+    piece = quarter // nk
+    ff = gate_weight.shape[2]
+    vmem = pl.BlockSpec(memory_space=pltpu.VMEM)
+    hbm = pl.BlockSpec(memory_space=pl.ANY)
+    dma = pltpu.SemaphoreType.DMA
+    slot_buf = pltpu.VMEM((nk, ep, slots, piece), BF16)
+    return pl.pallas_call(
+        functools.partial(fused_kernel, ep, nk, slots),
+        out_shape=jax.ShapeDtypeStruct((tok_rows, quarter), BF16),
+        in_specs=[vmem] * 4 + [hbm] * 3,
+        out_specs=vmem,
+        scratch_shapes=[
+            pltpu.VMEM((width, ff), BF16),
+            pltpu.VMEM((width, ff), BF16),
+            pltpu.VMEM((ff, width), BF16),
+            pltpu.VMEM((tok_rows, quarter), BF16),
+            pltpu.VMEM((ep * slots, tok_rows), F32),
+            pltpu.VMEM((tok_rows, ep * slots), BF16),
+            pltpu.VMEM((ep * slots, cap), BF16),
+            pltpu.VMEM((cap, ep * slots), BF16),
+            slot_buf,
+            slot_buf,
+            pltpu.VMEM((4, nk, cap, piece), BF16),
+            pltpu.VMEM((cap, ff), F32),
+            pltpu.VMEM((cap, ff), F32),
+            pltpu.VMEM((cap, ff), BF16),
+            pltpu.VMEM((nk, 2, cap, piece), BF16),
+            pltpu.VMEM((nk, 2, cap, piece), BF16),
+            pltpu.VMEM((nk, cap, piece), F32),
+            pltpu.VMEM((nk, cap, piece), BF16),
+            pltpu.VMEM((nk, cap, piece), BF16),
+            slot_buf,
+            slot_buf,
+            dma((6,)),
+            dma((nk, ep)),
+            dma((nk, ep)),
+        ]
+        + [dma((nk,))] * 10
+        + [dma((nk, ep))] * 2,
+        compiler_params=pltpu.CompilerParams(
+            collective_id=0, has_side_effects=True, vmem_limit_bytes=48 * 1024 * 1024
+        ),
+    )(tokens, norm_gain[None, :], chosen, route_weight, gate_weight, up_weight, down_weight)
+
+
 def solution(mesh):
+    small = mesh.shape["tp"] == 4
     return jax.shard_map(
-        shards,
+        fused if small else shards,
         mesh=mesh,
         in_specs=(
             P("ep", None),

time: 125 us -> 49.4 us (0.40)
  waiting for transfers between devices: 65.9 us -> 0 us
  Pallas kernels: 0 us -> 42.9 us
  between operations: 13.6 us -> 0.01 us
  starting transfers between devices: 12.8 us -> 0 us
  matrix products: 11.5 us -> 0 us
  other arithmetic: 10.5 us -> 0 us
  local copies, waits for them, and re-layouts: 10 us -> 6.19 us
    pallas_call x0 -> x1, Pallas kernels: none -> 42.9 us  [fused(): pl.pallas_call(functools.partial(fused_kernel, ep, nk, slots), out_shape=...]
    all_to_all x2 -> x0, waiting for transfers between devices: 42.2 us -> none  [the longest x1 31 us: shards(): lax.all_to_all(outgoing, 'ep', split_axis=0, concat_axis=0, tiled=True)]
    reduce_scatter x1 -> x0, waiting for transfers between devices: 23.7 us -> none  [shards(): lax.psum_scatter(lax.dot_general(down_mat, hidden, (((0,), (1,)), ((), ()...]
    all_to_all x2 -> x0, starting transfers between devices: 12.8 us -> none  [the longest x1 7.28 us: shards(): lax.all_to_all(outgoing, 'ep', split_axis=0, concat_axis=0, tiled=True)]
    dot_general x3 -> x0, matrix products: 11.5 us -> none  [the longest x1 7.02 us: shards(): lax.dot_general(down_mat, hidden, (((0,), (1,)), ((), ())), preferred_ele...]
    gather x7 -> x0, local copies, waits for them, and re-layouts: 9.46 us -> none  [the longest x3 2.91 us: shards(): slot_token = jnp.take_along_axis(chosen, slot_place, axis=1) - first_token]
    unnamed x8 -> x11, local copies, waits for them, and re-layouts: 0.02 us -> 6.19 us
    gather x7 -> x0, other arithmetic: 5.15 us -> none  [the longest x3 5.05 us: shards(): src_start[source_block]]
  transfers between devices with their start and end apart: 3 -> 0, of which waited for: 3 -> 0; matrix products, arithmetic and copies ran while one was open for 5% -> 0% of each run, Pallas kernels for 0% -> 0%
where the time goes in v1:
time: 49.4 us; the launch traced here: 49.1 us
  Pallas kernels  42.9 us (87%)
  local copies, waits for them, and re-layouts  6.19 us (13%)
    pallas_call x1, Pallas kernels, fused(): pl.pallas_call(functools.partial(fused_kernel, ep, nk, slots), out_shape=...  42.9 us
    unnamed x11, local copies, waits for them, and re-layouts  6.19 us

profile of v1, /device:TPU:0, one launch (start us, length us, event | category | flops | bytes accessed | tf_op | source)
XLA Modules:
  0.0 49.1 jit_solution(9199696544167768040)
XLA Ops:
  0.0 0.0 copy-start
  0.0 2.2 %copy-done = bf16[1,2048,1024]{2,1,0:T(8,128)(2,1)S(1)} copy-done((bf16[1,2048,1024]{2,1,0:T(8,128)(2,1)S(1)}, bf16[1,2048,1024]{2,1,0:T(8,128)(2,1)}, u32[]{:S(2)}) %copy-start) | copy-done | bytes 4194328
  2.2 0.0 copy-start.1
  2.2 1.2 %copy-done.1 = bf16[256,2048]{1,0:T(8,128)(2,1)S(1)} copy-done((bf16[256,2048]{1,0:T(8,128)(2,1)S(1)}, bf16[256,2048]{1,0:T(8,128)(2,1)}, u32[]{:S(2)}) %copy-start.1) | copy-done | bytes 1048600
  3.4 0.0 copy-start.2
  3.4 0.7 %copy-done.2 = f32[2048]{0:T(1024)S(1)} copy-done((f32[2048]{0:T(1024)S(1)}, f32[2048]{0:T(1024)}, u32[]{:S(2)}) %copy-start.2) | copy-done | bytes 8216
  4.1 0.0 copy-start.3
  4.1 0.7 %copy-done.3 = s32[8,256]{1,0:T(8,128)S(1)} copy-done((s32[8,256]{1,0:T(8,128)S(1)}, s32[8,256]{1,0:T(8,128)}, u32[]{:S(2)}) %copy-start.3) | copy-done | bytes 8216
  4.8 0.0 copy-start.4
  4.8 0.7 %copy-done.4 = f32[1,256]{1,0:T(1,128)S(1)} copy-done((f32[1,256]{1,0:T(1,128)S(1)}, f32[1,256]{1,0:T(1,128)}, u32[]{:S(2)}) %copy-start.4) | copy-done | bytes 1048
  5.5 42.9 %shard_map.73 = bf16[256,512]{1,0:T(8,128)(2,1)S(1)} custom-call(bf16[256,2048]{1,0:T(8,128)(2,1)S(1)} %copy-done.1, f32[1,2048]{1,0:T(1,128)S(1)} %bitcast.1, s32[8,256]{1,0:T(8,128)S(1)} %copy-done.3, f32[1,256]{1,0:T(1,128)S(1)} %copy-done.4, bf16[1,2048,1024]{2,1,0:T(8,128)(2,1)S(1)} %copy-done, bf16[1,2048,1024]{2,1,0:T(8,128)(2,1)} %up_hbm.1, ...), custom_call_target="tpu_custom_call" | custom-call | tf_op jit(solution)/shard_map/pallas_call | solution.py:293
  48.4 0.7 %copy.9 = bf16[256,512]{1,0:T(8,128)(2,1)} copy(bf16[256,512]{1,0:T(8,128)(2,1)S(1)} %shard_map.73) | data formatting | bytes 524288
Async XLA Ops:
  0.0 2.2 %copy-start = (bf16[1,2048,1024]{2,1,0:T(8,128)(2,1)S(1)}, bf16[1,2048,1024]{2,1,0:T(8,128)(2,1)}, u32[]{:S(2)}) copy-start(bf16[1,2048,1024]{2,1,0:T(8,128)(2,1)} %gate_hbm.1) | copy-start | bytes 12582916
  2.2 1.2 %copy-start.1 = (bf16[256,2048]{1,0:T(8,128)(2,1)S(1)}, bf16[256,2048]{1,0:T(8,128)(2,1)}, u32[]{:S(2)}) copy-start(bf16[256,2048]{1,0:T(8,128)(2,1)} %tokens.1) | copy-start | bytes 3145732
  3.4 0.7 %copy-start.2 = (f32[2048]{0:T(1024)S(1)}, f32[2048]{0:T(1024)}, u32[]{:S(2)}) copy-start(f32[2048]{0:T(1024)} %param.8) | copy-start | bytes 24580
  4.1 0.7 %copy-start.3 = (s32[8,256]{1,0:T(8,128)S(1)}, s32[8,256]{1,0:T(8,128)}, u32[]{:S(2)}) copy-start(s32[8,256]{1,0:T(8,128)} %chosen.1) | copy-start | bytes 24580
  4.8 0.7 %copy-start.4 = (f32[1,256]{1,0:T(1,128)S(1)}, f32[1,256]{1,0:T(1,128)}, u32[]{:S(2)}) copy-start(f32[1,256]{1,0:T(1,128)} %route.1) | copy-start | bytes 3076

commit v2 on v1

v2 whole, which is shorter than its diff:
```python
import functools
import jax
import jax.numpy as jnp
from jax import lax
from jax.experimental import pallas as pl
from jax.experimental.pallas import tpu as pltpu
from jax.sharding import PartitionSpec as P

F32 = jnp.float32
BF16 = jnp.bfloat16
MESH = pl.DeviceIdType.MESH
CUTS_IN = (4, 2, 2)
CUTS_OUT = (2, 2, 4)

def shards(tokens, norm_gain, chosen, route_weight, gate_weight, up_weight, down_weight):
    tok_rows, row_width = tokens.shape
    experts, capacity = chosen.shape
    ep_count = lax.axis_size("ep")
    tp_count = lax.axis_size("tp")
    owner_index = lax.axis_index("ep")
    slot_most = 3 * tok_rows // 16
    col_width = row_width // tp_count
    values = tokens.astype(jnp.float32)
    scale = lax.rsqrt(jnp.mean(values * values, axis=-1, keepdims=True) + 1e-06)
    normed = (values * scale * norm_gain[None, :]).astype(jnp.bfloat16)
    slot_steps = jnp.arange(slot_most, dtype=jnp.int32)
    first_token = owner_index * tok_rows
    run_start = jnp.sum((chosen < first_token).astype(jnp.int32), axis=1)
    run_end = jnp.sum((chosen < first_token + tok_rows).astype(jnp.int32), axis=1)
    run_count = run_end - run_start
    slot_live = slot_steps[None, :] < run_count[:, None]
    slot_place = jnp.minimum(run_start[:, None] + slot_steps[None, :], capacity - 1)
    slot_token = jnp.take_along_axis(chosen, slot_place, axis=1) - first_token
    slot_local = jnp.where(slot_live, slot_token, 0)
    my_chosen = lax.dynamic_index_in_dim(chosen, owner_index, 0, keepdims=False)
    block_edges = jnp.arange(ep_count, dtype=jnp.int32) * tok_rows
    src_start = jnp.sum((my_chosen[None, :] < block_edges[:, None]).astype(jnp.int32), axis=1)
    src_end = jnp.concatenate([src_start[1:], jnp.full((1,), capacity, jnp.int32)])
    gate_mat = gate_weight[0]
    up_mat = up_weight[0]
    down_mat = down_weight[0]
    outgoing = jnp.where(slot_live[:, :, None], normed[slot_local], jnp.zeros((), jnp.bfloat16))
    received = lax.all_to_all(outgoing, "ep", split_axis=0, concat_axis=0, tiled=True)
    source_block = my_chosen // tok_rows
    flat_index = (
        source_block * slot_most + jnp.arange(capacity, dtype=jnp.int32) - src_start[source_block]
    )
    expert_rows = received.reshape(-1, row_width)[flat_index]
    gate_pre = jnp.dot(expert_rows, gate_mat, preferred_element_type=jnp.float32)
    up_pre = jnp.dot(expert_rows, up_mat, preferred_element_type=jnp.float32)
    hidden = (jax.nn.silu(gate_pre) * up_pre).astype(jnp.bfloat16)
    summed_out = lax.psum_scatter(
        lax.dot_general(
            down_mat, hidden, (((0,), (1,)), ((), ())), preferred_element_type=jnp.float32
        ).astype(jnp.bfloat16),
        "tp",
        scatter_dimension=0,
        tiled=True,
    ).astype(jnp.float32)
    weighted = (summed_out.T * route_weight[0][:, None]).astype(jnp.bfloat16)
    back_place = jnp.minimum(src_start[:, None] + slot_steps[None, :], capacity - 1)
    back_live = slot_steps[None, :] < (src_end - src_start)[:, None]
    outgoing_back = jnp.where(
        back_live[:, :, None], weighted[back_place], jnp.zeros((), jnp.bfloat16)
    )
    returned = lax.all_to_all(outgoing_back, "ep", split_axis=0, concat_axis=0, tiled=True)
    target_row = jnp.where(slot_live, slot_token, tok_rows).reshape(-1)
    placement = (jnp.arange(tok_rows, dtype=jnp.int32)[:, None] == target_row[None, :]).astype(
        jnp.bfloat16
    )
    combined = jnp.dot(
        placement, returned.reshape(-1, col_width), preferred_element_type=jnp.float32
    )
    return combined.astype(jnp.bfloat16)


def fused_kernel(
    ep, slots, cuts_in, cuts_out,
    tokens_hbm, gain_hbm, chosen_hbm, route_hbm, gate_hbm, up_hbm, down_hbm, out,
    tokens, gain, chosen, route,
    gate_w, up_w, down_w, normed, pick, unpick, spread, gather, gate_acc, up_acc, hidden,
    outgoing, received, rows, pair_out, pair_in, own_part, cross_out, cross_in, back_out, back_in,
    in_sem, w_sem, ep_send, ep_recv, y_send, y_recv, pair_send, pair_recv, relay_send, relay_recv,
    ps_send, ps_recv, ys_send, ys_recv, back_send, back_recv,
):
    me = lax.axis_index("ep")
    tp = lax.axis_index("tp")
    y_pos = tp // 2
    core = tp % 2
    mate = y_pos * 2 + (1 - core)
    across = (1 - y_pos) * 2 + core
    diag = (1 - y_pos) * 2 + (1 - core)
    tok_rows, width = tokens.shape
    cap = chosen.shape[1]
    quarter = width // 4
    ff = gate_w.shape[1]
    order = [d for d in sorted(range(1, ep), key=lambda d: abs(d - ep / 2))]

    barrier = pltpu.get_barrier_semaphore()
    for d in order:
        pl.semaphore_signal(
            barrier, inc=1, device_id={"ep": (me + d) % ep, "tp": tp}, device_id_type=MESH
        )
    for other in (mate, across):
        pl.semaphore_signal(barrier, inc=1, device_id={"ep": me, "tp": other}, device_id_type=MESH)

    small = [
        pltpu.make_async_copy(a, b, in_sem.at[i])
        for i, (a, b) in enumerate(
            [(tokens_hbm, tokens), (gain_hbm, gain), (chosen_hbm, chosen), (route_hbm, route)]
        )
    ]
    for load in small:
        load.start()
    half = width // 2
    loads = []
    for i in range(2):
        part = pl.ds(i * half, half)
        loads.append(pltpu.make_async_copy(gate_hbm.at[0, part], gate_w.at[part], w_sem.at[3 * i]))
        loads.append(pltpu.make_async_copy(up_hbm.at[0, part], up_w.at[part], w_sem.at[3 * i + 1]))
    loads.append(pltpu.make_async_copy(down_hbm.at[0], down_w, w_sem.at[2]))
    for load in loads:
        load.start()
    for load in small:
        load.wait()

    first = me * tok_rows
    lane = lax.broadcasted_iota(jnp.int32, (slots, cap), 1).astype(F32)
    sub = lax.broadcasted_iota(jnp.int32, (slots, cap), 0).astype(F32)
    tok_lane = lax.broadcasted_iota(jnp.int32, (slots, tok_rows), 1).astype(F32)
    for e in range(ep):
        row = chosen[e : e + 1, :]
        local = (row - first).astype(F32)
        start = jnp.sum(jnp.where(local < 0.0, 1.0, 0.0), axis=1, keepdims=True)
        value = jnp.where((local >= 0.0) & (local < float(tok_rows)), local + 1.0, 0.0)
        hit = lane == sub + start
        slot_tok = jnp.sum(jnp.where(hit, value, 0.0), axis=1, keepdims=True) - 1.0
        pick[e * slots : (e + 1) * slots, :] = jnp.where(tok_lane == slot_tok, 1.0, 0.0)

    my_cols = pl.ds(pl.multiple_of(tp * quarter, quarter), quarter)
    my_gain = gain[:, my_cols]
    step_rows = 32

    @pl.loop(0, tok_rows // step_rows)
    def _(r):
        rs = pl.ds(pl.multiple_of(r * step_rows, step_rows), step_rows)
        v = tokens[rs, :].astype(F32)
        scale = lax.rsqrt(jnp.sum(v * v, axis=1, keepdims=True) * (1.0 / width) + 1e-06)
        own = tokens[rs, my_cols].astype(F32)
        normed[rs, :] = (own * scale * my_gain).astype(BF16)

    pick_b = pick[...].astype(BF16)
    for k, (off, size) in enumerate(cuts_in):
        got = jnp.dot(pick_b, normed[:, off : off + size], preferred_element_type=F32)
        outgoing[k][...] = got.astype(BF16).reshape(ep, slots, size)

    pl.semaphore_wait(barrier, ep + 1)

    def ep_copy(buf_out, buf_in, s_sem, r_sem, k, d):
        dest = (me + d) % ep
        return pltpu.make_async_remote_copy(
            src_ref=buf_out[k].at[dest], dst_ref=buf_in[k].at[me],
            send_sem=s_sem.at[k, d], recv_sem=r_sem.at[k, d],
            device_id={"ep": dest, "tp": tp}, device_id_type=MESH,
        )

    def tp_copy(a, b, s_sem, r_sem, k, other):
        return pltpu.make_async_remote_copy(
            src_ref=a, dst_ref=b, send_sem=s_sem.at[k], recv_sem=r_sem.at[k],
            device_id={"ep": me, "tp": other}, device_id_type=MESH,
        )

    sends = []

    def go(c):
        c.start()
        sends.append(c)

    n_in = len(cuts_in)
    dispatch = [
        [ep_copy(outgoing, received, ep_send, ep_recv, k, d) for d in order] for k in range(n_in)
    ]
    for k in range(n_in):
        for c in dispatch[k]:
            go(c)
    for k in range(n_in):
        received[k][me] = outgoing[k][me]

    mine = chosen[pl.ds(me, 1), :].astype(F32)
    place = lax.broadcasted_iota(jnp.int32, (1, cap), 1).astype(F32)
    slot_id = jnp.zeros((1, cap), F32)
    for b in range(ep):
        lo = float(b * tok_rows)
        begin = jnp.sum(jnp.where(mine < lo, 1.0, 0.0), axis=1, keepdims=True)
        inside = (mine >= lo) & (mine < lo + float(tok_rows))
        slot_id = jnp.where(inside, place - begin + float(b * slots), slot_id)
    slot_sub = lax.broadcasted_iota(jnp.int32, (ep * slots, cap), 0).astype(F32)
    spread_f = jnp.where(slot_sub == slot_id, 1.0, 0.0)
    spread[...] = spread_f.astype(BF16)
    gather[...] = spread_f.T.astype(BF16)
    unpick[...] = pick[...].T.astype(BF16)
    eye_r = lax.broadcasted_iota(jnp.int32, (cap, cap), 0)
    eye_c = lax.broadcasted_iota(jnp.int32, (cap, cap), 1)
    weight = jnp.sum(jnp.where(eye_r == eye_c, route[...], 0.0), axis=1, keepdims=True)

    def compact(k):
        size = cuts_in[k][1]
        for c in dispatch[k]:
            c.wait_recv()
        got = jnp.dot(
            gather[...], received[k][...].reshape(ep * slots, size), preferred_element_type=F32
        )
        mine_k = rows[k].at[tp]
        mine_k[...] = got.astype(BF16)
        go(tp_copy(mine_k, mine_k, y_send, y_recv, k, across))
        go(tp_copy(mine_k, mine_k, pair_send, pair_recv, k, mate))

    def relay(k):
        there = rows[k].at[across]
        tp_copy(rows[k].at[tp], there, y_send, y_recv, k, across).wait_recv()
        go(tp_copy(there, there, relay_send, relay_recv, k, mate))

    def project(near, far, opening=False, closing=False):
        for k in near:
            tp_copy(rows[k].at[tp], rows[k].at[mate], pair_send, pair_recv, k, mate).wait_recv()
        for k in far:
            tp_copy(rows[k].at[tp], rows[k].at[diag], relay_send, relay_recv, k, mate).wait_recv()
        work = [(k, t) for k in near for t in (tp, mate)] + [(k, t) for k in far for t in (across, diag)]
        tile = 256

        @pl.loop(0, ff // tile)
        def _(n):
            cols = pl.ds(pl.multiple_of(n * tile, tile), tile)
            g = None if opening else gate_acc[:, cols]
            u = None if opening else up_acc[:, cols]
            for k, t in work:
                off, size = cuts_in[k]
                ks = pl.ds(pl.multiple_of(t * quarter + off, 128), size)
                x = rows[k][t]
                dg = jnp.dot(x, gate_w[ks, cols], preferred_element_type=F32)
                du = jnp.dot(x, up_w[ks, cols], preferred_element_type=F32)
                g = dg if g is None else g + dg
                u = du if u is None else u + du
            if closing:
                hidden[:, cols] = (g / (1.0 + jnp.exp(-g)) * u).astype(BF16)
            else:
                gate_acc[:, cols] = g
                up_acc[:, cols] = u

    compact(0)
    compact(1)
    for load in loads[:4]:
        load.wait()
    project([0], [], opening=True)
    compact(2)
    relay(0)
    relay(1)
    project([1], [0])
    relay(2)
    project([2], [1])
    project([], [2], closing=True)
    loads[4].wait()

    def down(t, k):
        off, size = cuts_out[k]
        cols = pl.ds(pl.multiple_of(t * quarter + off, 128), size)
        return jnp.dot(hidden[...], down_w[:, cols], preferred_element_type=F32)

    n_out = len(cuts_out)
    pair_c = [tp_copy(pair_out[k], pair_in[k], ps_send, ps_recv, k, mate) for k in range(n_out)]
    cross_c = [tp_copy(cross_out[k], cross_in[k], ys_send, ys_recv, k, across) for k in range(n_out)]
    back = [
        [ep_copy(back_out, back_in, back_send, back_recv, k, d) for d in order] for k in range(n_out)
    ]

    def give(k):
        pair_out[k][0] = down(diag, k).astype(BF16)
        pair_out[k][1] = down(mate, k).astype(BF16)
        go(pair_c[k])

    def keep(k):
        own_part[k][0] = down(across, k)
        own_part[k][1] = down(tp, k)

    def cross(k):
        pair_c[k].wait_recv()
        cross_out[k][...] = (own_part[k][0] + pair_in[k][0].astype(F32)).astype(BF16)
        go(cross_c[k])

    def back_send_all(k):
        size = cuts_out[k][1]
        near = own_part[k][1] + pair_in[k][1].astype(F32)
        cross_c[k].wait_recv()
        total = (near + cross_in[k][...].astype(F32)) * weight
        wide = jnp.dot(spread[...], total.astype(BF16), preferred_element_type=F32)
        back_out[k][...] = wide.astype(BF16).reshape(ep, slots, size)
        for c in back[k]:
            go(c)
        back_in[k][me] = back_out[k][me]

    give(0)
    keep(0)
    for k in range(1, n_out):
        give(k)
        cross(k - 1)
        keep(k)
    cross(n_out - 1)
    for k in range(n_out):
        back_send_all(k)
    for k, (off, size) in enumerate(cuts_out):
        for c in back[k]:
            c.wait_recv()
        done = jnp.dot(
            unpick[...], back_in[k][...].reshape(ep * slots, size), preferred_element_type=F32
        )
        out[:, off : off + size] = done.astype(BF16)
    for c in sends:
        c.wait_send()


def cut(quarter, eighths):
    sizes = [quarter * e // 8 for e in eighths]
    return [(sum(sizes[:i]), size) for i, size in enumerate(sizes)]


def fused(tokens, norm_gain, chosen, route_weight, gate_weight, up_weight, down_weight):
    ep = lax.axis_size("ep")
    tok_rows, width = tokens.shape
    cap = chosen.shape[1]
    slots = 3 * tok_rows // 16
    quarter = width // lax.axis_size("tp")
    ff = gate_weight.shape[2]
    cuts_in = cut(quarter, CUTS_IN)
    cuts_out = cut(quarter, CUTS_OUT)
    hbm = pl.BlockSpec(memory_space=pl.ANY)
    dma = pltpu.SemaphoreType.DMA

    def bufs(cuts, lead, dtype=BF16):
        return [pltpu.VMEM(lead + (size,), dtype) for _, size in cuts]

    n_in, n_out = len(cuts_in), len(cuts_out)
    return pl.pallas_call(
        functools.partial(fused_kernel, ep, slots, cuts_in, cuts_out),
        out_shape=jax.ShapeDtypeStruct((tok_rows, quarter), BF16),
        in_specs=[hbm] * 7,
        out_specs=pl.BlockSpec(memory_space=pltpu.VMEM),
        scratch_shapes=[
            pltpu.VMEM((tok_rows, width), BF16),
            pltpu.VMEM((1, width), F32),
            pltpu.VMEM(chosen.shape, jnp.int32),
            pltpu.VMEM((1, cap), F32),
            pltpu.VMEM((width, ff), BF16),
            pltpu.VMEM((width, ff), BF16),
            pltpu.VMEM((ff, width), BF16),
            pltpu.VMEM((tok_rows, quarter), BF16),
            pltpu.VMEM((ep * slots, tok_rows), F32),
            pltpu.VMEM((tok_rows, ep * slots), BF16),
            pltpu.VMEM((ep * slots, cap), BF16),
            pltpu.VMEM((cap, ep * slots), BF16),
            pltpu.VMEM((cap, ff), F32),
            pltpu.VMEM((cap, ff), F32),
            pltpu.VMEM((cap, ff), BF16),
            bufs(cuts_in, (ep, slots)),
            bufs(cuts_in, (ep, slots)),
            bufs(cuts_in, (4, cap)),
            bufs(cuts_out, (2, cap)),
            bufs(cuts_out, (2, cap)),
            bufs(cuts_out, (2, cap), F32),
            bufs(cuts_out, (cap,)),
            bufs(cuts_out, (cap,)),
            bufs(cuts_out, (ep, slots)),
            bufs(cuts_out, (ep, slots)),
            dma((4,)),
            dma((5,)),
            dma((n_in, ep)),
            dma((n_in, ep)),
        ]
        + [dma((n_in,))] * 6
        + [dma((n_out,))] * 4
        + [dma((n_out, ep))] * 2,
        compiler_params=pltpu.CompilerParams(
            collective_id=0, has_side_effects=True, vmem_limit_bytes=60 * 1024 * 1024
        ),
    )(tokens, norm_gain[None, :], chosen, route_weight, gate_weight, up_weight, down_weight)


def solution(mesh):
    small = mesh.shape["tp"] == 4
    return jax.shard_map(
        fused if small else shards,
        mesh=mesh,
        in_specs=(
            P("ep", None),
            P(),
            P(),
            P("ep", None),
            P("ep", None, "tp"),
            P("ep", None, "tp"),
            P("ep", "tp", None),
        ),
        out_specs=P("ep", "tp"),
        check_vma=False,
    )
```

time: 49.4 us -> 46.3 us (0.937)
  local copies, waits for them, and re-layouts: 6.19 us -> 1.67 us
  Pallas kernels: 42.9 us -> 44.5 us
    unnamed x11 -> x1, local copies, waits for them, and re-layouts: 6.19 us -> 1.67 us
    pallas_call x1, Pallas kernels: 42.9 us -> 44.5 us  [fused(): pl.pallas_call(functools.partial(fused_kernel, ep, slots, cuts_in, cuts_o...]
where the time goes in v2:
time: 46.3 us; the launch traced here: 46.2 us
  Pallas kernels  44.5 us (96%)
  local copies, waits for them, and re-layouts  1.67 us (4%)
    pallas_call x1, Pallas kernels, fused(): pl.pallas_call(functools.partial(fused_kernel, ep, slots, cuts_in, cuts_o...  44.5 us
    unnamed x1, local copies, waits for them, and re-layouts  1.67 us

profile of v2, /device:TPU:0, one launch (start us, length us, event | category | flops | bytes accessed | tf_op | source)
XLA Modules:
  0.0 46.2 jit_solution(9397039110194448243)
XLA Ops:
  0.0 44.5 %shard_map.73 = bf16[256,512]{1,0:T(8,128)(2,1)} custom-call(bf16[256,2048]{1,0:T(8,128)(2,1)} %tokens_hbm.1, f32[1,2048]{1,0:T(1,128)} %bitcast.1, s32[8,256]{1,0:T(8,128)} %chosen_hbm.1, f32[1,256]{1,0:T(1,128)} %route_hbm.1, bf16[1,2048,1024]{2,1,0:T(8,128)(2,1)} %gate_hbm.1, bf16[1,2048,1024]{2,1,0:T(8,128)(2,1)} %up_hbm.1, bf16[1,1024,2048]{2,1,0:T(8,128)(2,1)} %down_hbm.1), custom_call_target="tpu_custom_call" | custom-call | tf_op jit(solution)/shard_map/pallas_call | solution.py:342
  44.5 1.7 %copy.9 = bf16[256,512]{1,0:T(8,128)(2,1)} copy(bf16[256,512]{1,0:T(8,128)(2,1)} %shard_map.73) | data formatting | bytes 524288

commit v3 on v2

--- a/solution.py
+++ b/solution.py
@@ -9,7 +9,7 @@
 F32 = jnp.float32
 BF16 = jnp.bfloat16
 MESH = pl.DeviceIdType.MESH
-CUTS_IN = (4, 2, 2)
+CUTS_IN = (2, 4, 2)
 CUTS_OUT = (2, 2, 4)
 
 def shards(tokens, norm_gain, chosen, route_weight, gate_weight, up_weight, down_weight):
@@ -110,7 +110,7 @@
             [(tokens_hbm, tokens), (gain_hbm, gain), (chosen_hbm, chosen), (route_hbm, route)]
         )
     ]
-    for load in small:
+    for load in (small[2], small[0], small[1], small[3]):
         load.start()
     half = width // 2
     loads = []
@@ -119,9 +119,7 @@
         loads.append(pltpu.make_async_copy(gate_hbm.at[0, part], gate_w.at[part], w_sem.at[3 * i]))
         loads.append(pltpu.make_async_copy(up_hbm.at[0, part], up_w.at[part], w_sem.at[3 * i + 1]))
     loads.append(pltpu.make_async_copy(down_hbm.at[0], down_w, w_sem.at[2]))
-    for load in loads:
-        load.start()
-    for load in small:
+    for load in small[2:]:
         load.wait()
 
     first = me * tok_rows
@@ -137,6 +135,10 @@
         slot_tok = jnp.sum(jnp.where(hit, value, 0.0), axis=1, keepdims=True) - 1.0
         pick[e * slots : (e + 1) * slots, :] = jnp.where(tok_lane == slot_tok, 1.0, 0.0)
 
+    pick_b = pick[...].astype(BF16)
+    for load in small[:2]:
+        load.wait()
+
     my_cols = pl.ds(pl.multiple_of(tp * quarter, quarter), quarter)
     my_gain = gain[:, my_cols]
     step_rows = 32
@@ -149,7 +151,6 @@
         own = tokens[rs, my_cols].astype(F32)
         normed[rs, :] = (own * scale * my_gain).astype(BF16)
 
-    pick_b = pick[...].astype(BF16)
     for k, (off, size) in enumerate(cuts_in):
         got = jnp.dot(pick_b, normed[:, off : off + size], preferred_element_type=F32)
         outgoing[k][...] = got.astype(BF16).reshape(ep, slots, size)
@@ -183,6 +184,8 @@
     for k in range(n_in):
         for c in dispatch[k]:
             go(c)
+    for load in loads:
+        load.start()
     for k in range(n_in):
         received[k][me] = outgoing[k][me]
 

time: 46.3 us -> 44.7 us (0.965)
  Pallas kernels: 44.5 us -> 42.8 us
    pallas_call x1, Pallas kernels: 44.5 us -> 42.8 us  [fused(): pl.pallas_call(functools.partial(fused_kernel, ep, slots, cuts_in, cuts_o...]
where the time goes in v3:
time: 44.7 us; the launch traced here: 44.5 us
  Pallas kernels  42.8 us (96%)
  local copies, waits for them, and re-layouts  1.67 us (4%)
    pallas_call x1, Pallas kernels, fused(): pl.pallas_call(functools.partial(fused_kernel, ep, slots, cuts_in, cuts_o...  42.8 us
    unnamed x1, local copies, waits for them, and re-layouts  1.67 us

profile of v3, /device:TPU:0, one launch (start us, length us, event | category | flops | bytes accessed | tf_op | source)
XLA Modules:
  0.0 44.5 jit_solution(9988213135718322275)
XLA Ops:
  0.0 42.8 %shard_map.73 = bf16[256,512]{1,0:T(8,128)(2,1)} custom-call(bf16[256,2048]{1,0:T(8,128)(2,1)} %tokens_hbm.1, f32[1,2048]{1,0:T(1,128)} %bitcast.1, s32[8,256]{1,0:T(8,128)} %chosen_hbm.1, f32[1,256]{1,0:T(1,128)} %route_hbm.1, bf16[1,2048,1024]{2,1,0:T(8,128)(2,1)} %gate_hbm.1, bf16[1,2048,1024]{2,1,0:T(8,128)(2,1)} %up_hbm.1, bf16[1,1024,2048]{2,1,0:T(8,128)(2,1)} %down_hbm.1), custom_call_target="tpu_custom_call" | custom-call | tf_op jit(solution)/shard_map/pallas_call | solution.py:345
  42.8 1.7 %copy.9 = bf16[256,512]{1,0:T(8,128)(2,1)} copy(bf16[256,512]{1,0:T(8,128)(2,1)} %shard_map.73) | data formatting | bytes 524288
